TPU v7x, 256 devices: a whole 4x4x8 slice. The times are simulated.
256 devices in a mesh: sp: 16 (over y, x), tp: 16 (over z, core).
Axes of the slice: x: 4, y: 4, z: 8, core: 2. Of those that a mesh axis runs over, the one named last changes fastest.
Arguments:
- query_a: bfloat16 [4096, 16, 256], P('sp', 'tp'), may hold values from -5.5 to 5.5
- key_a: bfloat16 [4096, 16, 256], P('sp', 'tp'), may hold values from -5.5 to 5.5
- value_a: bfloat16 [4096, 16, 256], P('sp', 'tp'), may hold values from -6 to 6
- query_b: bfloat16 [4096, 16, 128], P('sp', 'tp'), may hold values from -5.5 to 5.5
- key_b: bfloat16 [4096, 16, 128], P('sp', 'tp'), may hold values from -5.5 to 5.5
- value_b: bfloat16 [4096, 16, 128], P('sp', 'tp'), may hold values from -6 to 6
- lambdas: float32 [2, 16], P(None, 'tp'), may hold values from 0.3 to 0.8
- gain_a: float32 [256], replicated, may hold values from 0.1 to 1.9
- gain_b: float32 [128], replicated, may hold values from 0.1 to 1.9
- out_a: bfloat16 [4096, 4096], P('tp'), may hold values from -0.078125 to 0.078125
- out_b: bfloat16 [2048, 4096], P('tp'), may hold values from -0.078125 to 0.078125
- residual: bfloat16 [4096, 4096], P(('sp', 'tp')), may hold values from -6 to 6
- norm_gain: float32 [4096], replicated, may hold values from 0.1 to 1.9
- route_ids: int32 [4096, 2], P(('sp', 'tp')), may hold values from 0 to 31, all different within a row; in each aligned block of 16 rows (0 to 15, 16 to 31, ...) at most 2 rows name the same one
- route_weights: float32 [4096, 2], P(('sp', 'tp')), may hold values from 0.1 to 0.9
- w_gate: bfloat16 [32, 4096, 2048], P('sp', None, 'tp'), may hold values from -0.28125 to 0.28125
- w_up: bfloat16 [32, 4096, 2048], P('sp', None, 'tp'), may hold values from -0.28125 to 0.28125
- w_down: bfloat16 [32, 2048, 4096], P('sp', 'tp'), may hold values from -0.01977539 to 0.01977539
Outputs:
- result: bfloat16 [4096, 4096], P(('sp', 'tp'))
Inputs may be any that keep to these rules, and one draw needn't show every extreme that they name: `route_ids`: in the rows of one device each token names 2 different experts, no expert is named more than 2 times, a bound that some block reaches.
All inputs are finite; a program needn't handle non-finite values.
Results may differ from a plain program's by a relative error of at most 0.02.
Values may be sent and summed in bfloat16 or wider, within the bound.
No kernel may reach another device: no remote copies, remote signals or barrier semaphores. Data moves between devices by JAX's collectives and lax.ppermute only.
A program may use at most 128 MiB of HBM per device.

v0:
```python
import jax
import jax.numpy as jnp
from jax import lax
from jax.sharding import Mesh
from jax.sharding import PartitionSpec as P

TP = ("tp_0", "tp_1")
SP_TP = ("sp", "tp_0", "tp_1")
EPSILON = 1e-06
LIMIT = 7.0
SLOPE = 1.702
FLOOR = -1e30


def sent_together(arrays, axis, dim, along):
    both = jnp.concatenate(arrays, axis=along)
    out, at, finished = (lax.all_gather(both, axis, axis=dim, tiled=True), 0, [])
    for a in arrays:
        finished.append(lax.slice_in_dim(out, at, at + a.shape[along], axis=along))
        at += a.shape[along]
    return tuple(finished)


def sum_in_order(tiles, axes, sequence):
    dims = [lax.axis_size(a) for a in axes]
    tiles = tiles.reshape(*dims, *tiles.shape[1:])
    tiles = tiles.transpose(*sequence, *range(len(axes), tiles.ndim))
    tiles = tiles.reshape(-1, *tiles.shape[len(axes) :])
    for k in sequence:
        tiles = lax.psum_scatter(tiles, axes[k], scatter_dimension=0, tiled=True)
    return tiles[0]


def in_blocks(array, dim, length):
    before, after = (array.shape[:dim], array.shape[dim + 1 :])
    return jnp.moveaxis(array.reshape(*before, length, -1, *after), dim, 0)


def sum_by_axis(array, axes, sequence, dim):
    length = lax.axis_size(axes)
    return sum_in_order(in_blocks(array, dim, length), axes, sequence)


def empty_state(heads_here, queries_here, value_width):
    maxima = jnp.full((2, heads_here, queries_here), FLOOR, jnp.float32)
    totals = jnp.zeros((2, heads_here, queries_here), jnp.float32)
    sums = jnp.zeros((2, heads_here, queries_here, value_width), jnp.float32)
    return (maxima, totals, sums)


def absorb_keys(states, queries, keys, values, width):
    maxima, totals, sums = states
    scaling = width ** (-0.5)
    new_maxima = []
    new_totals = []
    new_sums = []
    for which in range(2):
        query_part = queries[:, :, which * width : (which + 1) * width]
        key_part = keys[:, :, which * width : (which + 1) * width]
        scores = (
            jnp.einsum("qhd,khd->hqk", query_part, key_part, preferred_element_type=jnp.float32)
            * scaling
        )
        highest = jnp.maximum(maxima[which], jnp.max(scores, axis=2))
        expo = jnp.exp(scores - highest[:, :, None])
        factor = jnp.exp(maxima[which] - highest)
        new_totals.append(totals[which] * factor + jnp.sum(expo, axis=2))
        carried = jnp.einsum(
            "hqk,khv->hqv", expo.astype(jnp.bfloat16), values, preferred_element_type=jnp.float32
        )
        new_sums.append(sums[which] * factor[:, :, None] + carried)
        new_maxima.append(highest)
    return (jnp.stack(new_maxima), jnp.stack(new_totals), jnp.stack(new_sums))


def finish(states, lambda_row, gain):
    maxima, totals, sums = states
    heard = sums / totals[:, :, :, None]
    differ = heard[0] - lambda_row[:, None, None] * heard[1]
    scaled = lax.rsqrt(jnp.mean(differ * differ, axis=2, keepdims=True) + EPSILON)
    return (differ * scaled * gain).astype(jnp.bfloat16)


def gated_units(grid, w_gate, w_up):
    gate = jnp.einsum("necd,edf->necf", grid, w_gate, preferred_element_type=jnp.float32)
    upward = jnp.einsum("necd,edf->necf", grid, w_up, preferred_element_type=jnp.float32)
    clamped = jnp.minimum(gate, LIMIT)
    return (
        clamped * jax.nn.sigmoid(SLOPE * clamped) * (jnp.clip(upward, -LIMIT, LIMIT) + 1.0)
    ).astype(jnp.bfloat16)


def per_device(
    query_a,
    key_a,
    value_a,
    query_b,
    key_b,
    value_b,
    lambdas,
    gain_a,
    gain_b,
    out_a,
    out_b,
    residual,
    norm_gain,
    route_ids,
    route_weights,
    w_gate,
    w_up,
    w_down,
):
    heads_here = query_a.shape[1]
    queries_here = query_a.shape[0]
    width_a = query_a.shape[2] // 2
    width_b = query_b.shape[2] // 2
    starting = (
        empty_state(heads_here, queries_here, value_a.shape[2]),
        empty_state(heads_here, queries_here, value_b.shape[2]),
    )
    keys_a, values_a, keys_b, values_b = sent_together((key_a, value_a, key_b, value_b), "sp", 0, 2)
    state_a = absorb_keys(starting[0], query_a, keys_a, values_a, width_a)
    state_b = absorb_keys(starting[1], query_b, keys_b, values_b, width_b)
    attended_a = finish(state_a, lambdas[0], gain_a)
    attended_b = finish(state_b, lambdas[1], gain_b)
    model_width = out_a.shape[1]
    weights_a = out_a.reshape(heads_here, -1, model_width)
    weights_b = out_b.reshape(heads_here, -1, model_width)
    first = jnp.einsum("hqv,hvd->qd", attended_a, weights_a, preferred_element_type=jnp.float32)
    projected = lax.psum_scatter(
        (
            first
            + jnp.einsum("hqv,hvd->qd", attended_b, weights_b, preferred_element_type=jnp.float32)
        ).astype(jnp.bfloat16),
        TP,
        scatter_dimension=0,
        tiled=True,
    ).astype(jnp.float32)
    mixed = (residual.astype(jnp.float32) + projected).astype(jnp.bfloat16)
    widened = mixed.astype(jnp.float32)
    normed = (
        widened
        * lax.rsqrt(jnp.mean(widened * widened, axis=1, keepdims=True) + EPSILON)
        * norm_gain
    ).astype(jnp.bfloat16)
    rows_here, chosen = route_ids.shape
    groups = lax.axis_size("sp")
    experts_here = w_gate.shape[0]
    experts_all = experts_here * groups
    capacity = 2 * rows_here * chosen // experts_all
    slots_here = experts_here * capacity
    flat_ids = route_ids.reshape(-1)
    onehot = (flat_ids[:, None] == jnp.arange(experts_all, dtype=jnp.int32)[None, :]).astype(
        jnp.int32
    )
    earlier = jnp.cumsum(onehot, axis=0) - onehot
    target = flat_ids * capacity + jnp.sum(earlier * onehot, axis=1)
    places = jnp.arange(experts_all * capacity, dtype=jnp.int32)
    layout = jnp.any(target.reshape(rows_here, chosen)[None, :, :] == places[:, None, None], axis=2)
    outgoing = jnp.dot(
        layout.astype(jnp.bfloat16), normed, preferred_element_type=jnp.float32
    ).astype(jnp.bfloat16)
    outgoing = outgoing.reshape(groups, slots_here, model_width)
    arrived = lax.all_to_all(outgoing, "sp", split_axis=0, concat_axis=0, tiled=True)
    pieces = lax.all_gather(arrived, TP, axis=0, tiled=True)
    count = pieces.shape[0]
    grid = pieces.reshape(count, experts_here, capacity, model_width)
    active = gated_units(grid, w_gate, w_up)
    down = jnp.einsum("necf,efd->necd", active, w_down, preferred_element_type=jnp.float32)
    partial_value = down.astype(jnp.bfloat16).reshape(count, slots_here, model_width)
    totals = (
        sum_by_axis(partial_value.astype(jnp.float32).astype(jnp.bfloat16), TP, (1, 0), 0)
        .astype(jnp.float32)
        .astype(jnp.bfloat16)
    )
    summed = lax.all_to_all(totals, "sp", split_axis=0, concat_axis=0, tiled=True)
    results = summed.reshape(experts_all * capacity, model_width)
    picked = (
        jnp.take(results, target, axis=0)
        .reshape(rows_here, chosen, model_width)
        .astype(jnp.float32)
    )
    combined = jnp.sum(route_weights[:, :, None] * picked, axis=1)
    return (widened + combined).astype(jnp.bfloat16)


def solution(mesh):
    split = Mesh(mesh.devices.reshape(mesh.shape["sp"], 8, 2), ("sp", "tp_0", "tp_1"))
    placed = (
        P("sp", TP, None),
        P("sp", TP, None),
        P("sp", TP, None),
        P("sp", TP, None),
        P("sp", TP, None),
        P("sp", TP, None),
        P(None, TP),
        P(),
        P(),
        P(TP, None),
        P(TP, None),
        P(SP_TP, None),
        P(),
        P(SP_TP, None),
        P(SP_TP, None),
        P("sp", None, TP),
        P("sp", None, TP),
        P("sp", TP, None),
    )
    return jax.shard_map(
        per_device, mesh=split, in_specs=placed, out_specs=P(SP_TP, None), check_vma=False
    )
```

profile of v0, /device:TPU:1, one launch (start us, length us, event | category | flops | bytes accessed | tf_op | source)
XLA Modules:
  0.0 375.3 jit_solution(6805099216005470352)
XLA Ops:
  6.5 2.0 pad_maximum_fusion
  8.6 1.4 fusion.127
  10.0 69.7 %all-gather.3.cloned.1.call-done = bf16[4096,1,768]{2,0,1:T(8,128)(2,1)} async-done(((bf16[256,1,768]{2,0,1:T(8,128)(2,1)}), bf16[4096,1,768]{2,0,1:T(8,128)(2,1)}) %all-gather.3.cloned.1.call-update) | async-done | bytes 6291472 | tf_op jit(solution)/shard_map/all_gather | solution.py:17
  79.7 2.2 fusion.131
  84.4 1.2 fusion.52
  85.5 1.2 fusion.58
  89.0 0.9 fusion.128
  92.3 0.9 multiply_reduce_fusion.2
  93.2 1.5 fusion.101
  94.8 2.9 fusion
  98.6 56.4 %reduce-scatter.4.cloned.1.call-done = bf16[16,4096]{1,0:T(8,128)(2,1)} async-done(((bf16[256,4096]{1,0:T(8,128)(2,1)}), bf16[16,4096]{1,0:T(8,128)(2,1)}) %reduce-scatter.4.cloned.1.call-update) | async-done | bytes 131088 | tf_op jit(solution)/shard_map/reduce_scatter | solution.py:130
  155.0 1.1 fusion.79
  156.1 1.3 convolution_convert_fusion.1
  157.5 15.3 %all_to_all.10 = bf16[16,4,4096]{2,1,0:T(4,128)(2,1)} all-to-all(bf16[16,4,4096]{2,1,0:T(4,128)(2,1)S(1)} %reshape.633), channel_id=1, replica_groups=mesh['sp'=16,'tp_0'=8,'tp_1'=2] {'sp'}, dimensions={0} | all-to-all | bytes 1048576 | tf_op jit(solution)/shard_map/all_to_all | solution.py:164
  172.9 56.6 %all-gather.5.cloned.1.call-done = bf16[256,4,4096]{2,1,0:T(4,128)(2,1)} async-done(((bf16[16,4,4096]{2,1,0:T(4,128)(2,1)}), bf16[256,4,4096]{2,1,0:T(4,128)(2,1)}) %all-gather.5.cloned.1.call-update) | async-done | bytes 8388624 | tf_op jit(solution)/shard_map/all_gather | solution.py:165
  229.6 11.3 %copy.46 = bf16[256,4,4096]{2,0,1:T(8,128)(2,1)} copy(bf16[256,4,4096]{2,1,0:T(4,128)(2,1)} %all-gather.5.cloned.1.call-done) | data formatting | bytes 16777216 | tf_op jit(solution)/shard_map/all_gather | solution.py:165
  240.9 5.7 %fusion.29 = f32[256,2,2,128]{3,0,2,1:T(8,128)S(1)} fusion(bf16[256,2,2,4096]{3,0,2,1:T(8,128)(2,1)} %bitcast.148, bf16[2,4096,128]{2,1,0:T(8,128)(2,1)S(1)} %copy-done.3), kind=kOutput, calls=%fused_computation.36 | convolution fusion | flops 1073872896 | bytes 11010048 | tf_op jit(solution)/shard_map/necd,edf->necf/dot_general | solution.py:85
  246.7 13.4 %convolution_convert_fusion = bf16[2,256,2,4096]{3,1,2,0:T(8,128)(2,1)} fusion(bf16[2,128,4096]{2,1,0:T(8,128)(2,1)S(1)} %copy-done, bf16[256,2,2,4096]{3,0,2,1:T(8,128)(2,1)} %bitcast.149, bf16[2,4096,128]{2,1,0:T(8,128)(2,1)} %param.34, f32[256,2,2,128]{3,0,2,1:T(8,128)S(1)} %fusion.29), kind=kOutput, calls=%fused_computation.1 | convolution fusion | flops 2152857600 | bytes 21495808 | tf_op jit(solution)/shard_map/necf,efd->necd/dot_general | solution.py:169
  260.1 7.7 %copy.47 = bf16[8,2,16,4,4096]{4,2,3,0,1:T(8,128)(2,1)} copy(bf16[8,2,16,4,4096]{4,2,1,0,3:T(8,128)(2,1)} %bitcast.151) | data formatting | bytes 16777216 | tf_op jit(solution)/shard_map/reshape;reshape | solution.py:26
  267.9 20.6 %reduce-scatter.6.cloned.1.call-done = bf16[8,16,4,4096]{3,1,2,0:T(8,128)(2,1)} async-done(((bf16[16,16,4,4096]{3,1,2,0:T(8,128)(2,1)}), bf16[8,16,4,4096]{3,1,2,0:T(8,128)(2,1)}) %reduce-scatter.6.cloned.1.call-update) | async-done | bytes 4194320 | tf_op jit(solution)/shard_map/reduce_scatter | solution.py:30
  288.5 58.4 %reduce-scatter.8.cloned.1.call-done = bf16[1,16,4,4096]{3,1,2,0:T(8,128)(2,1)} async-done(((bf16[8,16,4,4096]{3,1,2,0:T(8,128)(2,1)}), bf16[1,16,4,4096]{3,1,2,0:T(8,128)(2,1)}) %reduce-scatter.8.cloned.1.call-update) | async-done | bytes 524304 | tf_op jit(solution)/shard_map/reduce_scatter | solution.py:30
  346.9 2.2 copy.48
  349.2 6.5 %all-to-all-start.1 = ((bf16[16,4,4096]{2,1,0:T(4,128)(2,1)}), bf16[16,4,4096]{2,1,0:T(4,128)(2,1)S(1)}, u32[]{:S(2)}, u32[]{:S(2)}) async-start(bf16[16,4,4096]{2,1,0:T(4,128)(2,1)} %copy.48), calls=%async_computation.4 | async-start | bytes 1048576 | tf_op jit(solution)/shard_map/all_to_all | solution.py:176
  356.1 10.1 %all-to-all-done.1 = bf16[16,4,4096]{2,1,0:T(4,128)(2,1)S(1)} async-done(((bf16[16,4,4096]{2,1,0:T(4,128)(2,1)}), bf16[16,4,4096]{2,1,0:T(4,128)(2,1)S(1)}, u32[]{:S(2)}, u32[]{:S(2)}) %all-to-all-start.1) | async-done | bytes 524320 | tf_op jit(solution)/shard_map/all_to_all | solution.py:176
  (84 shorter events, 11.3 us)
Async XLA Ops:
  6.5 240.1 %copy-start = (bf16[2,128,4096]{2,1,0:T(8,128)(2,1)S(1)}, bf16[2,128,4096]{2,1,0:T(8,128)(2,1)}, u32[]{:S(2)}) copy-start(bf16[2,128,4096]{2,1,0:T(8,128)(2,1)} %param.35) | copy-start | bytes 6291460
  6.5 73.2 %all-gather.3.cloned.1.call-start = ((), (), s32[]{:S(2)}) async-start(), calls=%async_computation.5 | async-start | bytes 6684672 | tf_op jit(solution)/shard_map/all_gather | solution.py:17
  8.5 146.5 %reduce-scatter.4.cloned.1.call-start = ((), (), s32[]{:S(2)}) async-start(), calls=%async_computation.6 | async-start | bytes 2228224 | tf_op jit(solution)/shard_map/reduce_scatter | solution.py:130
  10.0 72.6 %copy-start.8 = (bf16[256,1,256]{2,0,1:T(8,128)(2,1)S(1)}, bf16[256,1,256]{2,0,1:T(8,128)(2,1)}, u32[]{:S(2)}) copy-start(bf16[256,1,256]{2,0,1:T(8,128)(2,1)} %param.18) | copy-start | bytes 393220
  79.7 3.1 copy-start.1
  85.5 1.9 copy-start.7
  91.4 1.8 copy-start.6
  91.4 1.8 copy-start.11
  92.3 2.4 copy-start.2
  92.3 2.4 copy-start.12
  94.7 3.2 copy-start.10
  94.7 60.3 %copy-start.4 = (bf16[16,4096]{1,0:T(8,128)(2,1)S(1)}, bf16[16,4096]{1,0:T(8,128)(2,1)}, u32[]{:S(2)}) copy-start(bf16[16,4096]{1,0:T(8,128)(2,1)} %param.29) | copy-start | bytes 393220
  94.8 61.3 %copy-start.9 = (f32[4096]{0:T(1024)S(1)}, f32[4096]{0:T(1024)}, u32[]{:S(2)}) copy-start(f32[4096]{0:T(1024)} %param.30) | copy-start | bytes 49156
  97.6 131.9 %all-gather.5.cloned.1.call-start = ((), (), s32[]{:S(2)}) async-start(), calls=%async_computation.7 | async-start | bytes 8912896 | tf_op jit(solution)/shard_map/all_gather | solution.py:165
  172.9 115.6 %reduce-scatter.6.cloned.1.call-start = ((), (), s32[]{:S(2)}) async-start(), calls=%async_computation.8 | async-start | bytes 12582912 | tf_op jit(solution)/shard_map/reduce_scatter | solution.py:30
  229.6 11.3 %copy-start.3 = (bf16[2,4096,128]{2,1,0:T(8,128)(2,1)S(1)}, bf16[2,4096,128]{2,1,0:T(8,128)(2,1)}, u32[]{:S(2)}) copy-start(bf16[2,4096,128]{2,1,0:T(8,128)(2,1)} %param.33) | copy-start | bytes 6291460
  267.8 88.2 %copy-start.13 = (f32[16,2]{0,1:T(2,128)S(1)}, f32[16,2]{0,1:T(2,128)}, u32[]{:S(2)}) copy-start(f32[16,2]{0,1:T(2,128)} %param.32) | copy-start | bytes 388
  267.8 79.1 %reduce-scatter.8.cloned.1.call-start = ((), (), s32[]{:S(2)}) async-start(), calls=%async_computation.9 | async-start | bytes 4718592 | tf_op jit(solution)/shard_map/reduce_scatter | solution.py:30
  288.5 79.5 %copy-start.5 = (bf16[16,4096]{1,0:T(8,128)(2,1)S(1)}, bf16[16,4096]{1,0:T(8,128)(2,1)}, u32[]{:S(2)}) copy-start(bf16[16,4096]{1,0:T(8,128)(2,1)} %reduce-scatter.4.cloned.1.call-done) | copy-start | bytes 393220
  349.2 17.0 %all-to-all-start.1 = ((bf16[16,4,4096]{2,1,0:T(4,128)(2,1)}), bf16[16,4,4096]{2,1,0:T(4,128)(2,1)S(1)}, u32[]{:S(2)}, u32[]{:S(2)}) async-start(bf16[16,4,4096]{2,1,0:T(4,128)(2,1)} %copy.48), calls=%async_computation.4 | async-start | bytes 1048576 | tf_op jit(solution)/shard_map/all_to_all | solution.py:176
Sparse Core Ops, SparseCore 0:
  9.8 69.8 all-gather.2
  97.8 57.1 reduce-scatter.3
  173.0 56.5 all-gather.4
  267.9 20.5 reduce-scatter.5
  290.9 55.9 reduce-scatter.7
where the time goes:
time: 376 us; the launch traced here: 375 us
  waiting for transfers between devices  272 us (72%)
  matrix products  33.6 us (9%)
  local copies, waits for them, and re-layouts  24.9 us (7%)
  blocking collectives  15.3 us (4%)
  between operations  13.5 us (4%)
  other arithmetic  9.25 us (2%)
  starting transfers between devices  6.87 us (2%)
    reduce_scatter x2, waiting for transfers between devices, sum_in_order(): tiles = lax.psum_scatter(tiles, axes[k], scatter_dimension=0, tiled=True)  79 us
    all_gather x1, waiting for transfers between devices, sent_together(): lax.all_gather(both, axis, axis=dim, tiled=True)  69.7 us
    all_gather x1, waiting for transfers between devices, per_device(): pieces = lax.all_gather(arrived, TP, axis=0, tiled=True)  56.6 us
    reduce_scatter x1, waiting for transfers between devices, per_device(): lax.psum_scatter((first + jnp.einsum('hqv,hvd->qd', attended_b, weights_b...  56.4 us
    all_to_all x1, blocking collectives, per_device(): lax.all_to_all(outgoing, 'sp', split_axis=0, concat_axis=0, tiled=True)  15.3 us
    dot_general x1, matrix products, per_device(): jnp.einsum('necf,efd->necd', active, w_down, preferred_element_type=jnp.f...  13.4 us
    all_gather x1, local copies, waits for them, and re-layouts, per_device(): pieces = lax.all_gather(arrived, TP, axis=0, tiled=True)  11.3 us
    all_to_all x1, waiting for transfers between devices, per_device(): lax.all_to_all(totals, 'sp', split_axis=0, concat_axis=0, tiled=True)  10.1 us
  transfers between devices with their start and end apart: 6, of which 6 were waited for; matrix products, arithmetic and copies ran while one was open for 1% of the time, Pallas kernels for 0%

commit v1 on v0

--- a/solution.py
+++ b/solution.py
@@ -162,7 +162,9 @@
     ).astype(jnp.bfloat16)
     outgoing = outgoing.reshape(groups, slots_here, model_width)
     arrived = lax.all_to_all(outgoing, "sp", split_axis=0, concat_axis=0, tiled=True)
-    pieces = lax.all_gather(arrived, TP, axis=0, tiled=True)
+    pieces = jnp.concatenate(
+        lax.all_to_all(jnp.stack([arrived] * lax.axis_size(TP)), TP, 0, 0), axis=0
+    )
     count = pieces.shape[0]
     grid = pieces.reshape(count, experts_here, capacity, model_width)
     active = gated_units(grid, w_gate, w_up)

time: 376 us -> 508 us (1.35)
  blocking collectives: 15.3 us -> 211 us
  waiting for transfers between devices: 272 us -> 210 us
    all_to_all x0 -> x1, blocking collectives: none -> 196 us  [per_device(): lax.all_to_all(jnp.stack([arrived] * lax.axis_size(TP)), TP, 0, 0)]
    all_gather x1 -> x0, waiting for transfers between devices: 56.6 us -> none  [per_device(): pieces = lax.all_gather(arrived, TP, axis=0, tiled=True)]
    all_gather x1 -> x0, local copies, waits for them, and re-layouts: 11.3 us -> none  [per_device(): pieces = lax.all_gather(arrived, TP, axis=0, tiled=True)]
    all_to_all x0 -> x2, local copies, waits for them, and re-layouts: none -> 8.15 us  [the longest x1 7.86 us: per_device(): lax.all_to_all(jnp.stack([arrived] * lax.axis_size(TP)), TP, 0, 0)]
    reduce_scatter x2, waiting for transfers between devices: 79 us -> 73.8 us  [sum_in_order(): tiles = lax.psum_scatter(tiles, axes[k], scatter_dimension=0, tiled=True)]
  transfers between devices with their start and end apart: 6 -> 5, of which waited for: 6 -> 5; matrix products, arithmetic and copies ran while one was open for 1% -> 0% of each run, Pallas kernels for 0% -> 0%
where the time goes in v1:
time: 508 us; the launch traced here: 507 us
  blocking collectives  211 us (42%)
  waiting for transfers between devices  210 us (41%)
  matrix products  33.6 us (7%)
  local copies, waits for them, and re-layouts  22.8 us (4%)
  between operations  13.5 us (3%)
  other arithmetic  9.25 us (2%)
  starting transfers between devices  6.85 us (1%)
    all_to_all x1, blocking collectives, per_device(): lax.all_to_all(jnp.stack([arrived] * lax.axis_size(TP)), TP, 0, 0)  196 us
    reduce_scatter x2, waiting for transfers between devices, sum_in_order(): tiles = lax.psum_scatter(tiles, axes[k], scatter_dimension=0, tiled=True)  73.8 us
    all_gather x1, waiting for transfers between devices, sent_together(): lax.all_gather(both, axis, axis=dim, tiled=True)  69.7 us
    reduce_scatter x1, waiting for transfers between devices, per_device(): lax.psum_scatter((first + jnp.einsum('hqv,hvd->qd', attended_b, weights_b...  56.4 us
    all_to_all x1, blocking collectives, per_device(): lax.all_to_all(outgoing, 'sp', split_axis=0, concat_axis=0, tiled=True)  15.2 us
    dot_general x1, matrix products, per_device(): jnp.einsum('necf,efd->necd', active, w_down, preferred_element_type=jnp.f...  13.4 us
  transfers between devices with their start and end apart: 5, of which 5 were waited for; matrix products, arithmetic and copies ran while one was open for 0% of the time, Pallas kernels for 0%

profile of v1, /device:TPU:1, one launch (start us, length us, event | category | flops | bytes accessed | tf_op | source)
XLA Modules:
  0.0 507.2 jit_solution(2465910042576922622)
XLA Ops:
  6.5 2.0 pad_maximum_fusion
  8.6 1.4 fusion.127
  10.0 69.7 %all-gather.2.cloned.1.call-done = bf16[4096,1,768]{2,0,1:T(8,128)(2,1)} async-done(((bf16[256,1,768]{2,0,1:T(8,128)(2,1)}), bf16[4096,1,768]{2,0,1:T(8,128)(2,1)}) %all-gather.2.cloned.1.call-update) | async-done | bytes 6291472 | tf_op jit(solution)/shard_map/all_gather | solution.py:17
  79.7 2.2 fusion.131
  84.4 1.2 fusion.52
  85.5 1.2 fusion.58
  89.0 0.9 fusion.128
  93.2 1.5 fusion.101
  94.8 2.9 fusion
  98.6 56.4 %reduce-scatter.4.cloned.1.call-done = bf16[16,4096]{1,0:T(8,128)(2,1)} async-done(((bf16[256,4096]{1,0:T(8,128)(2,1)}), bf16[16,4096]{1,0:T(8,128)(2,1)}) %reduce-scatter.4.cloned.1.call-update) | async-done | bytes 131088 | tf_op jit(solution)/shard_map/reduce_scatter | solution.py:130
  155.0 1.1 fusion.79
  156.1 1.3 convolution_convert_fusion.1
  157.5 15.2 %all_to_all.15 = bf16[16,4,4096]{2,1,0:T(4,128)(2,1)S(1)} all-to-all(bf16[16,4,4096]{2,1,0:T(4,128)(2,1)S(1)} %reshape.632), channel_id=1, replica_groups=mesh['sp'=16,'tp_0'=8,'tp_1'=2] {'sp'}, dimensions={0} | all-to-all | bytes 1048576 | tf_op jit(solution)/shard_map/all_to_all | solution.py:164
  173.1 1.1 stack.26
  174.1 196.0 %all_to_all.16 = bf16[16,16,4,4096]{3,1,2,0:T(8,128)(2,1)} all-to-all(bf16[16,16,4,4096]{3,1,2,0:T(8,128)(2,1)S(1)} %stack.26), channel_id=1, replica_groups=mesh['sp'=16,'tp_0'=8,'tp_1'=2] {'tp_0','tp_1'}, dimensions={0} | all-to-all | bytes 16777216 | tf_op jit(solution)/shard_map/all_to_all | solution.py:166
  370.1 7.9 %copy.49 = bf16[16,16,4,4096]{3,1,0,2:T(8,128)(2,1)} copy(bf16[16,16,4,4096]{3,1,2,0:T(8,128)(2,1)} %all_to_all.16) | data formatting | bytes 16777216 | tf_op jit(solution)/shard_map/all_to_all | solution.py:166
  378.0 5.7 %fusion.29 = f32[256,2,2,128]{3,0,2,1:T(8,128)S(1)} fusion(bf16[256,2,2,4096]{3,0,2,1:T(8,128)(2,1)} %bitcast.148, bf16[2,4096,128]{2,1,0:T(8,128)(2,1)S(1)} %copy-done.3), kind=kOutput, calls=%fused_computation.36 | convolution fusion | flops 1073872896 | bytes 11010048 | tf_op jit(solution)/shard_map/necd,edf->necf/dot_general | solution.py:85
  383.7 13.4 %convolution_convert_fusion = bf16[2,256,2,4096]{3,1,2,0:T(8,128)(2,1)} fusion(bf16[2,128,4096]{2,1,0:T(8,128)(2,1)S(1)} %copy-done, bf16[256,2,2,4096]{3,0,2,1:T(8,128)(2,1)} %bitcast.149, bf16[2,4096,128]{2,1,0:T(8,128)(2,1)} %param.34, f32[256,2,2,128]{3,0,2,1:T(8,128)S(1)} %fusion.29), kind=kOutput, calls=%fused_computation.1 | convolution fusion | flops 2152857600 | bytes 21495808 | tf_op jit(solution)/shard_map/necf,efd->necd/dot_general | solution.py:171
  397.1 7.7 %copy.50 = bf16[8,2,16,4,4096]{4,2,3,0,1:T(8,128)(2,1)} copy(bf16[8,2,16,4,4096]{4,2,1,0,3:T(8,128)(2,1)} %bitcast.151) | data formatting | bytes 16777216 | tf_op jit(solution)/shard_map/reshape;reshape | solution.py:26
  404.9 15.4 %reduce-scatter.6.cloned.1.call-done = bf16[8,16,4,4096]{3,1,2,0:T(8,128)(2,1)} async-done(((bf16[16,16,4,4096]{3,1,2,0:T(8,128)(2,1)}), bf16[8,16,4,4096]{3,1,2,0:T(8,128)(2,1)}) %reduce-scatter.6.cloned.1.call-update) | async-done | bytes 4194320 | tf_op jit(solution)/shard_map/reduce_scatter | solution.py:30
  420.4 58.4 %reduce-scatter.8.cloned.1.call-done = bf16[1,16,4,4096]{3,1,2,0:T(8,128)(2,1)} async-done(((bf16[8,16,4,4096]{3,1,2,0:T(8,128)(2,1)}), bf16[1,16,4,4096]{3,1,2,0:T(8,128)(2,1)}) %reduce-scatter.8.cloned.1.call-update) | async-done | bytes 524304 | tf_op jit(solution)/shard_map/reduce_scatter | solution.py:30
  478.8 2.3 copy.51
  481.0 6.5 %all-to-all-start.2 = ((bf16[16,4,4096]{2,1,0:T(4,128)(2,1)}), bf16[16,4,4096]{2,1,0:T(4,128)(2,1)S(1)}, u32[]{:S(2)}, u32[]{:S(2)}) async-start(bf16[16,4,4096]{2,1,0:T(4,128)(2,1)} %copy.51), calls=%async_computation.5 | async-start | bytes 1048576 | tf_op jit(solution)/shard_map/all_to_all | solution.py:178
  488.0 10.1 %all-to-all-done.2 = bf16[16,4,4096]{2,1,0:T(4,128)(2,1)S(1)} async-done(((bf16[16,4,4096]{2,1,0:T(4,128)(2,1)}), bf16[16,4,4096]{2,1,0:T(4,128)(2,1)S(1)}, u32[]{:S(2)}, u32[]{:S(2)}) %all-to-all-start.2) | async-done | bytes 524320 | tf_op jit(solution)/shard_map/all_to_all | solution.py:178
  (84 shorter events, 12.4 us)
Async XLA Ops:
  6.5 377.2 %copy-start = (bf16[2,128,4096]{2,1,0:T(8,128)(2,1)S(1)}, bf16[2,128,4096]{2,1,0:T(8,128)(2,1)}, u32[]{:S(2)}) copy-start(bf16[2,128,4096]{2,1,0:T(8,128)(2,1)} %param.35) | copy-start | bytes 6291460
  6.5 73.2 %all-gather.2.cloned.1.call-start = ((), (), s32[]{:S(2)}) async-start(), calls=%async_computation.6 | async-start | bytes 6684672 | tf_op jit(solution)/shard_map/all_gather | solution.py:17
  8.5 146.5 %reduce-scatter.4.cloned.1.call-start = ((), (), s32[]{:S(2)}) async-start(), calls=%async_computation.7 | async-start | bytes 2228224 | tf_op jit(solution)/shard_map/reduce_scatter | solution.py:130
  10.0 72.6 %copy-start.8 = (bf16[256,1,256]{2,0,1:T(8,128)(2,1)S(1)}, bf16[256,1,256]{2,0,1:T(8,128)(2,1)}, u32[]{:S(2)}) copy-start(bf16[256,1,256]{2,0,1:T(8,128)(2,1)} %param.18) | copy-start | bytes 393220
  79.7 3.1 copy-start.1
  85.5 1.9 copy-start.7
  91.4 1.8 copy-start.6
  91.4 1.8 copy-start.11
  92.3 2.4 copy-start.2
  92.3 2.4 copy-start.12
  94.7 3.2 copy-start.10
  94.7 60.3 %copy-start.4 = (bf16[16,4096]{1,0:T(8,128)(2,1)S(1)}, bf16[16,4096]{1,0:T(8,128)(2,1)}, u32[]{:S(2)}) copy-start(bf16[16,4096]{1,0:T(8,128)(2,1)} %param.29) | copy-start | bytes 393220
  94.8 61.3 %copy-start.9 = (f32[4096]{0:T(1024)S(1)}, f32[4096]{0:T(1024)}, u32[]{:S(2)}) copy-start(f32[4096]{0:T(1024)} %param.30) | copy-start | bytes 49156
  97.6 322.7 %reduce-scatter.6.cloned.1.call-start = ((), (), s32[]{:S(2)}) async-start(), calls=%async_computation.8 | async-start | bytes 12582912 | tf_op jit(solution)/shard_map/reduce_scatter | solution.py:30
  370.1 7.9 %copy-start.3 = (bf16[2,4096,128]{2,1,0:T(8,128)(2,1)S(1)}, bf16[2,4096,128]{2,1,0:T(8,128)(2,1)}, u32[]{:S(2)}) copy-start(bf16[2,4096,128]{2,1,0:T(8,128)(2,1)} %param.33) | copy-start | bytes 6291460
  404.9 83.0 %copy-start.13 = (f32[16,2]{0,1:T(2,128)S(1)}, f32[16,2]{0,1:T(2,128)}, u32[]{:S(2)}) copy-start(f32[16,2]{0,1:T(2,128)} %param.32) | copy-start | bytes 388
  404.9 73.9 %reduce-scatter.8.cloned.1.call-start = ((), (), s32[]{:S(2)}) async-start(), calls=%async_computation.9 | async-start | bytes 4718592 | tf_op jit(solution)/shard_map/reduce_scatter | solution.py:30
  420.4 79.5 %copy-start.5 = (bf16[16,4096]{1,0:T(8,128)(2,1)S(1)}, bf16[16,4096]{1,0:T(8,128)(2,1)}, u32[]{:S(2)}) copy-start(bf16[16,4096]{1,0:T(8,128)(2,1)} %reduce-scatter.4.cloned.1.call-done) | copy-start | bytes 393220
  481.0 17.0 %all-to-all-start.2 = ((bf16[16,4,4096]{2,1,0:T(4,128)(2,1)}), bf16[16,4,4096]{2,1,0:T(4,128)(2,1)S(1)}, u32[]{:S(2)}, u32[]{:S(2)}) async-start(bf16[16,4,4096]{2,1,0:T(4,128)(2,1)} %copy.51), calls=%async_computation.5 | async-start | bytes 1048576 | tf_op jit(solution)/shard_map/all_to_all | solution.py:178
Sparse Core Ops, SparseCore 0:
  9.8 69.8 all-gather.1
  97.8 57.1 reduce-scatter.3
  405.0 15.3 reduce-scatter.5
  422.8 55.9 reduce-scatter.7
